TPU v7x, 128 devices: a whole 4x4x4 slice. The times are simulated.
128 devices in a mesh: ep: 128 (over z, y, x, core).
Axes of the slice: x: 4, y: 4, z: 4, core: 2. Of those that a mesh axis runs over, the one named last changes fastest.
Arguments:
- tokens: bfloat16 [512, 2048], P('ep'), may hold values from -6 to 6
- lengths: int32 [512], P('ep'), may hold values from 1 to 1023
- cache_keys: bfloat16 [512, 1024, 2, 128], P('ep')
- cache_values: bfloat16 [512, 1024, 2, 128], P('ep'), may hold values from -6 to 6
- query_w: bfloat16 [2048, 1024], replicated, may hold values from -0.125 to 0.125
- key_w: bfloat16 [2048, 256], replicated, may hold values from -0.125 to 0.125
- value_w: bfloat16 [2048, 256], replicated, may hold values from -0.125 to 0.125
- out_w: bfloat16 [1024, 2048], replicated, may hold values from -0.1875 to 0.1875
- mix_lambda: float32 [8], replicated, may hold values from 0.3 to 0.8
- head_gain: float32 [128], replicated, may hold values from 0.1 to 1.9
- attn_gain: float32 [2048], replicated, may hold values from 0.1 to 1.9
- ffn_gain: float32 [2048], replicated, may hold values from 0.1 to 1.9
- routes: int32 [512, 2], P('ep'), may hold values from 0 to 7, all different within a row; in each aligned block of 4 rows (0 to 3, 4 to 7, ...) at most 2 rows name the same one
- route_weights: float32 [512, 2], P('ep'), may hold values from 0.2 to 1
- exp_gate: bfloat16 [2048, 49152], P(None, 'ep'), may hold values from -0.125 to 0.125
- exp_up: bfloat16 [2048, 49152], P(None, 'ep'), may hold values from -0.125 to 0.125
- exp_down: bfloat16 [49152, 2048], P('ep'), may hold values from -0.078125 to 0.078125
- dense_gate: bfloat16 [128, 256, 352], P('ep'), may hold values from -0.125 to 0.125
- dense_up: bfloat16 [128, 256, 352], P('ep'), may hold values from -0.125 to 0.125
- dense_down: bfloat16 [128, 352, 256], P('ep'), may hold values from -0.078125 to 0.078125
- branch_gate: bfloat16 [2048], replicated, may hold values from -0.125 to 0.125
Outputs:
- output: bfloat16 [512, 2048], P('ep')
- new_keys: bfloat16 [512, 256], P('ep')
- new_values: bfloat16 [512, 256], P('ep')
Inputs may be any that keep to these rules, and one draw needn't show every extreme that they name: `routes`: each row names 2 different experts; among the 4 rows of one device no expert is named by more than 2 rows, a bound that some block reaches.
All inputs are finite; a program needn't handle non-finite values.
Results may differ from a plain program's by a relative error of at most 0.015.
Values may be sent and summed in bfloat16 or wider, within the bound.
A program may use at most 128 MiB of HBM per device.

v0:
```python
import functools

import jax
import jax.numpy as jnp
from jax import lax
from jax.experimental import pallas as pl
from jax.experimental.pallas import tpu as pltpu
from jax.sharding import PartitionSpec as P

HEADS = 8
KV_HEADS = 2
HEAD_DIM = 128
SPLIT = 16
SIDE = 128
QKV_CHUNKS = 4
ROW_CHUNK = 128

F32 = jnp.float32
BF16 = jnp.bfloat16
MESH = pl.DeviceIdType.MESH


def attention_part(
    experts,
    small,
    keys,
    values,
    query_w,
    key_w,
    value_w,
    out_w,
    ext,
    hidden,
    new_keys,
    new_values,
    kbuf,
    vbuf,
    qbuf,
    kwbuf,
    vwbuf,
    obuf,
    qscr,
    hscr,
    wsem,
    ksem,
    vsem,
    osem,
    more_loads,
):
    tokens, lengths, lam, head_gain, attn_gain, ffn_gain, routes, route_weights, branch_gate = [
        dst for _, dst in small[0]
    ]
    rows, width = tokens.shape
    span = keys.shape[1]
    step = width // QKV_CHUNKS
    groups = HEADS // KV_HEADS
    half = HEAD_DIM // 2
    small_copies = [
        pltpu.make_async_copy(src, dst, small[1].at[i]) for i, (src, dst) in enumerate(small[0])
    ]
    for copy in small_copies:
        copy.start()
    weight_copies = []
    for c in range(QKV_CHUNKS):
        part = pl.ds(c * step, step)
        trio = [
            pltpu.make_async_copy(src.at[part], dst.at[part], wsem.at[3 * c + i])
            for i, (src, dst) in enumerate(((query_w, qbuf), (key_w, kwbuf), (value_w, vwbuf)))
        ]
        for copy in trio:
            copy.start()
        weight_copies.append(trio)
    key_copies = [pltpu.make_async_copy(keys.at[s], kbuf.at[s], ksem.at[s]) for s in range(rows)]
    value_copies = [pltpu.make_async_copy(values.at[s], vbuf.at[s], vsem.at[s]) for s in range(rows)]
    for s in range(rows):
        key_copies[s].start()
        value_copies[s].start()
    out_copy = pltpu.make_async_copy(out_w, obuf, osem.at[0])
    out_copy.start()
    for copy in more_loads:
        copy.start()
    for copy in small_copies:
        copy.wait()

    x = tokens[...].astype(F32)
    normed = x * lax.rsqrt(jnp.mean(x * x, axis=-1, keepdims=True) + 1e-06) * attn_gain[...]
    normed = normed.astype(BF16)
    query = jnp.zeros((rows, query_w.shape[1]), F32)
    knew = jnp.zeros((rows, key_w.shape[1]), F32)
    vnew = jnp.zeros((rows, value_w.shape[1]), F32)
    for c in range(QKV_CHUNKS):
        for copy in weight_copies[c]:
            copy.wait()
        part = slice(c * step, (c + 1) * step)
        left = normed[:, part]
        query += jnp.dot(left, qbuf[part, :], preferred_element_type=F32)
        knew += jnp.dot(left, kwbuf[part, :], preferred_element_type=F32)
        vnew += jnp.dot(left, vwbuf[part, :], preferred_element_type=F32)
    new_keys[...] = knew.astype(BF16)
    new_values[...] = vnew.astype(BF16)
    query = query.astype(BF16).astype(F32)
    knew = knew.astype(BF16).astype(F32)
    vnew = vnew.astype(BF16).astype(F32)
    for s in range(rows):
        for h in range(HEADS):
            qscr[s, h : h + 1, :] = query[s : s + 1, h * HEAD_DIM : (h + 1) * HEAD_DIM]

    scale = half ** (-0.5)
    lane = lax.broadcasted_iota(jnp.int32, (HEADS, HEAD_DIM), 1)
    head_row = lax.broadcasted_iota(jnp.int32, (HEADS, HEAD_DIM), 0)
    col = lax.broadcasted_iota(jnp.int32, (2 * HEADS, span), 1)
    row = lax.broadcasted_iota(jnp.int32, (2 * HEADS, span), 0)
    own_group = (col % KV_HEADS) == ((row % HEADS) // groups)
    head_col = lax.broadcasted_iota(jnp.int32, (HEADS, 1), 0)
    lam_col = jnp.zeros((HEADS, 1), F32)
    for h in range(HEADS):
        lam_col = jnp.where(head_col == h, lam[h], lam_col)
    for s in range(rows):
        q = qscr[s]
        both = jnp.concatenate([jnp.where(lane < half, q, 0.0), jnp.where(lane >= half, q, 0.0)], axis=0)
        kown = jnp.zeros((HEADS, HEAD_DIM), F32)
        vown = jnp.zeros((HEADS, HEAD_DIM), F32)
        for g in range(KV_HEADS):
            mine = head_row // groups == g
            part = slice(g * HEAD_DIM, (g + 1) * HEAD_DIM)
            kown = jnp.where(mine, knew[s : s + 1, part], kown)
            vown = jnp.where(mine, vnew[s : s + 1, part], vown)
        own = jnp.sum(both * jnp.concatenate([kown, kown], axis=0), axis=-1, keepdims=True) * scale
        key_copies[s].wait()
        scores = lax.dot_general(
            both.astype(BF16), kbuf[s], (((1,), (1,)), ((), ())), preferred_element_type=F32
        ) * scale
        valid = own_group & (col < KV_HEADS * lengths[s])
        largest = jnp.maximum(
            jnp.max(jnp.where(valid, scores, -jnp.inf), axis=-1, keepdims=True), own
        )
        raised = jnp.where(valid, jnp.exp(scores - largest), 0.0)
        own_raised = jnp.exp(own - largest)
        inverse = 1.0 / (jnp.sum(raised, axis=-1, keepdims=True) + own_raised)
        prob = raised * inverse
        own_prob = own_raised * inverse
        weights = (prob[:HEADS] - lam_col * prob[HEADS:]).astype(BF16)
        own_weights = (own_prob[:HEADS] - lam_col * own_prob[HEADS:]).astype(BF16).astype(F32)
        value_copies[s].wait()
        mixed = jnp.dot(weights, vbuf[s], preferred_element_type=F32) + own_weights * vown
        normal = mixed * lax.rsqrt(jnp.mean(mixed * mixed, axis=-1, keepdims=True) + 1e-05)
        normal = normal * head_gain[...]
        for h in range(HEADS):
            hscr[s : s + 1, h * HEAD_DIM : (h + 1) * HEAD_DIM] = normal[h : h + 1, :]
    out_copy.wait()
    state = x + jnp.dot(hscr[...].astype(BF16), obuf[...], preferred_element_type=F32)
    hidden[...] = state
    ffn = state * lax.rsqrt(jnp.mean(state * state, axis=-1, keepdims=True) + 1e-06)
    ffn = (ffn * ffn_gain[...]).astype(BF16)
    ext[:, :width] = ffn
    pieces = jnp.zeros((rows, SIDE), F32)
    branch = branch_gate[...].astype(F32)
    for c in range(width // SIDE):
        pieces += ffn[:, c * SIDE : (c + 1) * SIDE].astype(F32) * branch[c : c + 1, :]
    logit = jnp.sum(pieces, axis=-1, keepdims=True)
    gate = 1.0 / (1.0 + jnp.exp(-logit))
    spot = lax.broadcasted_iota(jnp.int32, (rows, SIDE), 1)
    name = spot % (SIDE // 2)
    table = jnp.where(name == experts, gate, 0.0)
    token_row = lax.broadcasted_iota(jnp.int32, (rows, SIDE), 0)
    for k in range(routes.shape[0]):
        for s in range(rows):
            here = (name == routes[k, s]) & (name < experts) & (token_row == s)
            table = table + jnp.where(here, route_weights[k, s], 0.0)
    high = table.astype(BF16).astype(F32)
    ext[:, width:] = jnp.where(spot < SIDE // 2, high, table - high).astype(BF16)


def layer_kernel(
    n,
    tokens,
    lengths,
    lam,
    head_gain,
    attn_gain,
    ffn_gain,
    routes,
    route_weights,
    branch_gate,
    keys,
    values,
    query_w,
    key_w,
    value_w,
    out_w,
    exp_gate,
    exp_up,
    exp_down,
    dense_gate,
    dense_up,
    dense_down,
    out,
    new_keys,
    new_values,
    tokens_v,
    lengths_v,
    lam_v,
    head_gain_v,
    attn_gain_v,
    ffn_gain_v,
    routes_v,
    route_weights_v,
    branch_gate_v,
    small_sem,
    ext,
    hidden,
    kbuf,
    vbuf,
    qbuf,
    kwbuf,
    vwbuf,
    obuf,
    qscr,
    hscr,
    asem,
    ksem,
    vsem,
    osem,
    egbuf,
    eubuf,
    edbuf,
    dgbuf,
    dubuf,
    ddbuf,
    recv,
    xall,
    gpart,
    upart,
    gsend,
    usend,
    grecv,
    urecv,
    act,
    total,
    sib_send,
    sib_recv,
    rs_send,
    rs_recv,
    wsem,
    ag_send_sem,
    ag_recv_sem,
    fw_send_sem,
    fw_recv_sem,
    ex_send_sem,
    ex_recv_sem,
    sib_send_sem,
    sib_recv_sem,
    rs_send_sem,
    rs_recv_sem,
):
    me = lax.axis_index("ep")
    chips = n // 2
    chip, core = me // 2, lax.rem(me, 2)
    sibling = chip * 2 + 1 - core
    blocks = n // SPLIT
    experts = n // SPLIT
    rows, width = hidden.shape
    total_rows = n * rows
    chunk = min(ROW_CHUNK, total_rows)
    row_span = dense_gate.shape[2]

    def at(k):
        return lax.rem(chip + k, chips) * 2 + core

    gchips = SPLIT // 2
    block = me // SPLIT
    expert = me // SPLIT
    gchip = lax.rem(me, SPLIT) // 2
    group_rows = SPLIT * rows

    def mate(j):
        return block * SPLIT + lax.rem(gchip + j, gchips) * 2 + core

    def group(d):
        return lax.rem(block + d, blocks)

    def place(d, j):
        return group(d) * gchips + lax.rem(gchip + j, gchips)

    def source(b, j):
        home = lax.rem(block + blocks - b, blocks)
        return home * SPLIT + lax.rem(gchip + gchips - j, gchips) * 2 + core

    loads = [
        pltpu.make_async_copy(src, dst, wsem.at[i])
        for i, (src, dst) in enumerate(
            (
                (dense_gate.at[0], dgbuf),
                (dense_up.at[0], dubuf),
                (exp_gate, egbuf),
                (exp_up, eubuf),
                (exp_down, edbuf),
                (dense_down.at[0], ddbuf),
            )
        )
    ]
    barrier = pltpu.get_barrier_semaphore()

    def greet(k, carry):
        pl.semaphore_signal(barrier, inc=1, device_id=(at(k),), device_id_type=MESH)
        return carry

    lax.fori_loop(1, chips, greet, 0)
    pl.semaphore_signal(barrier, inc=1, device_id=(sibling,), device_id_type=MESH)
    small = [
        (tokens, tokens_v),
        (lengths, lengths_v),
        (lam, lam_v),
        (head_gain, head_gain_v),
        (attn_gain, attn_gain_v),
        (ffn_gain, ffn_gain_v),
        (routes, routes_v),
        (route_weights, route_weights_v),
        (branch_gate, branch_gate_v),
    ]
    attention_part(
        experts, (small, small_sem), keys, values, query_w, key_w, value_w, out_w, ext, hidden,
        new_keys, new_values, kbuf, vbuf, qbuf, kwbuf, vwbuf, obuf, qscr, hscr,
        asem, ksem, vsem, osem, loads,
    )
    pl.semaphore_wait(barrier, chips)

    def send_block(ref, owner, q, target):
        return pltpu.make_async_remote_copy(
            src_ref=ref,
            dst_ref=recv.at[owner],
            send_sem=ag_send_sem.at[q],
            recv_sem=ag_recv_sem.at[q],
            device_id=(target,),
            device_id_type=MESH,
        )

    def near_copy(j):
        return send_block(ext, me, j, mate(j))

    def far_copy(b):
        return send_block(ext, me, b * gchips, group(b) * SPLIT + lax.rem(me, SPLIT))

    def relay_copy(b, j):
        owner = source(b, 0)
        return send_block(recv.at[owner], owner, b * gchips + j, mate(j))

    def fw_copy(b, j):
        owner = source(b, j)
        return pltpu.make_async_remote_copy(
            src_ref=recv.at[owner],
            dst_ref=recv.at[owner],
            send_sem=fw_send_sem.at[b * gchips + j],
            recv_sem=fw_recv_sem.at[b * gchips + j],
            device_id=(sibling,),
            device_id_type=MESH,
        )

    own_copy = pltpu.make_async_remote_copy(
        src_ref=ext,
        dst_ref=recv.at[me],
        send_sem=fw_send_sem.at[0],
        recv_sem=fw_recv_sem.at[0],
        device_id=(sibling,),
        device_id_type=MESH,
    )

    def loop(low, high, body):
        def run(i, carry):
            body(i)
            return carry

        lax.fori_loop(low, high, run, 0)

    for b in range(1, blocks):
        far_copy(b).start()
    loop(1, gchips, lambda j: near_copy(j).start())
    own_copy.start()
    recv[me] = ext[...]
    for b in range(1, blocks):
        far_copy(b).wait_recv()
        loop(1, gchips, lambda j: relay_copy(b, j).start())
        fw_copy(b, 0).start()

    def near_forward(j):
        near_copy(j).wait_recv()
        fw_copy(0, j).start()

    loop(1, gchips, near_forward)
    own_copy.wait_recv()
    loop(1, gchips, lambda j: fw_copy(0, j).wait_recv())

    def widen(home):
        def one(i):
            c = home * gchips + i
            pair = jnp.concatenate([recv[2 * c].astype(F32), recv[2 * c + 1].astype(F32)], axis=0)
            xall[pl.ds(pl.multiple_of(c * 2 * rows, 2 * rows), 2 * rows), :] = pair

        loop(0, gchips, one)

    def group_part(d):
        return pl.ds(pl.multiple_of(group(d) * group_rows, group_rows), group_rows)

    def by_rows(body):
        if total_rows == chunk:
            body(pl.ds(0, chunk))
        else:

            def run(r, carry):
                body(pl.ds(pl.multiple_of(r * chunk, chunk), chunk))
                return carry

            lax.fori_loop(0, total_rows // chunk, run, 0)

    loads[0].wait()
    loads[1].wait()

    def dense_in(part):
        left = xall[part, pl.ds(pl.multiple_of(block * row_span, 128), row_span)].astype(BF16)
        across = (((1,), (1,)), ((), ()))
        g = lax.dot_general(left, dgbuf[...], across, preferred_element_type=F32)
        u = lax.dot_general(left, dubuf[...], across, preferred_element_type=F32)
        gpart[part, :] = g
        upart[part, :] = u
        gsend[part, :] = g.astype(BF16)
        usend[part, :] = u.astype(BF16)

    def exchange(b):
        part = group_part(b)
        copies = []
        for j in range(1, blocks):
            for i, (src, dst) in enumerate(((gsend, grecv), (usend, urecv))):
                slot = 2 * (b * (blocks - 1) + j - 1) + i
                copies.append(
                    pltpu.make_async_remote_copy(
                        src_ref=src.at[part],
                        dst_ref=dst.at[j - 1, part],
                        send_sem=ex_send_sem.at[slot],
                        recv_sem=ex_recv_sem.at[slot],
                        device_id=(lax.rem(me + j * SPLIT, n),),
                        device_id_type=MESH,
                    )
                )
        for copy in copies:
            copy.start()
        return copies

    widen(block)
    dense_in(group_part(0))
    exchanges = [exchange(0)]
    for b in range(1, blocks):

        def relay_forward(j):
            relay_copy(b, j).wait_recv()
            fw_copy(b, j).start()

        loop(1, gchips, relay_forward)
    for b in range(1, blocks):
        loop(0, gchips, lambda j: fw_copy(b, j).wait_recv())
    for b in range(1, blocks):
        widen(group(b))
        dense_in(group_part(b))
        exchanges.append(exchange(b))

    loads[2].wait()
    loads[3].wait()

    def expert_in(part):
        left = xall[part, :width].astype(BF16)
        g = jnp.dot(left, egbuf[...], preferred_element_type=F32)
        u = jnp.dot(left, eubuf[...], preferred_element_type=F32)
        act[part, :] = (g / (1.0 + jnp.exp(-g)) * u).astype(BF16)

    by_rows(expert_in)
    loads[4].wait()

    def side_value(part, which):
        side = xall[part, width:]
        spot = lax.broadcasted_iota(jnp.int32, side.shape, 1) % (SIDE // 2)
        return jnp.sum(jnp.where(spot == which, side, 0.0), axis=-1, keepdims=True)

    def expert_out(part):
        product = jnp.dot(act[part, :], edbuf[...], preferred_element_type=F32)
        total[part, :] = product * side_value(part, expert)

    by_rows(expert_out)
    loads[5].wait()

    def dense_out(part):
        g = gpart[part, :]
        u = upart[part, :]
        for j in range(blocks - 1):
            g = g + grecv[j, part, :].astype(F32)
            u = u + urecv[j, part, :].astype(F32)
        dact = (g / (1.0 + jnp.exp(-g)) * u).astype(BF16)
        product = jnp.dot(dact, ddbuf[...], preferred_element_type=F32)
        cols = pl.ds(pl.multiple_of(block * row_span, 128), row_span)
        total[part, cols] = total[part, cols] + product * side_value(part, experts)

    def both_halves(d, j):
        c = place(d, j)
        pair = total[pl.ds(pl.multiple_of(c * 2 * rows, 2 * rows), 2 * rows), :]
        return pair[:rows], pair[rows:]

    def sib_copy(q):
        return pltpu.make_async_remote_copy(
            src_ref=sib_send.at[q],
            dst_ref=sib_recv.at[q],
            send_sem=sib_send_sem.at[q],
            recv_sem=sib_recv_sem.at[q],
            device_id=(sibling,),
            device_id_type=MESH,
        )

    def rs_copy(d, j):
        q = d * gchips + j
        return pltpu.make_async_remote_copy(
            src_ref=rs_send.at[q],
            dst_ref=rs_recv.at[q],
            send_sem=rs_send_sem.at[q],
            recv_sem=rs_recv_sem.at[q],
            device_id=(place(d, j) * 2 + core,),
            device_id_type=MESH,
        )

    def add_sibling(d, j):
        q = d * gchips + j
        sib_copy(q).wait_recv()
        low, high = both_halves(d, j)
        return jnp.where(core == 0, low, high) + sib_recv[q].astype(F32)

    for d in list(range(1, blocks)) + [0]:
        for j in range(1, blocks):
            first = 2 * (j - 1)
            for copy in exchanges[(j + d) % blocks][first : first + 2]:
                copy.wait_recv()
        dense_out(group_part(d))

        def pack(j):
            low, high = both_halves(d, j)
            sib_send[d * gchips + j] = jnp.where(core == 0, high, low).astype(BF16)

        def forward(j):
            rs_send[d * gchips + j] = add_sibling(d, j).astype(BF16)
            rs_copy(d, j).start()

        loop(0, gchips, pack)
        loop(0, gchips, lambda j: sib_copy(d * gchips + j).start())
        loop(1 if d == 0 else 0, gchips, forward)
    result = hidden[...] + add_sibling(0, 0)

    def collect(q, acc):
        rs_copy(q // gchips, lax.rem(q, gchips)).wait_recv()
        return acc + rs_recv[q].astype(F32)

    result = lax.fori_loop(1, chips, collect, result)
    out[...] = result.astype(BF16)

    for b in range(1, blocks):
        far_copy(b).wait_send()
        loop(1, gchips, lambda j: relay_copy(b, j).wait_send())
        loop(0, gchips, lambda j: fw_copy(b, j).wait_send())
        loop(0, gchips, lambda j: rs_copy(b, j).wait_send())
    own_copy.wait_send()

    def drain(j):
        near_copy(j).wait_send()
        fw_copy(0, j).wait_send()
        rs_copy(0, j).wait_send()

    loop(1, gchips, drain)
    loop(0, chips, lambda q: sib_copy(q).wait_send())
    for copies in exchanges:
        for copy in copies:
            copy.wait_send()


def finish_kernel(count, *refs):
    sources, targets, held = refs[:count], refs[count : 2 * count], refs[2 * count : 3 * count]
    in_sem, out_sem = refs[3 * count :]
    ins = [pltpu.make_async_copy(sources[i], held[i], in_sem.at[i]) for i in range(count)]
    outs = [pltpu.make_async_copy(held[i], targets[i], out_sem.at[i]) for i in range(count)]
    for copy in ins:
        copy.start()
    for i in range(count):
        ins[i].wait()
        outs[i].start()
    for copy in outs:
        copy.wait()


def per_device(
    n,
    tokens,
    lengths,
    cache_keys,
    cache_values,
    query_w,
    key_w,
    value_w,
    out_w,
    mix_lambda,
    head_gain,
    attn_gain,
    ffn_gain,
    routes,
    route_weights,
    exp_gate,
    exp_up,
    exp_down,
    dense_gate,
    dense_up,
    dense_down,
    branch_gate,
):
    rows, width = tokens.shape
    cache_len = cache_keys.shape[1]
    span = cache_len * KV_HEADS
    experts = n // SPLIT
    vmem = pl.BlockSpec(memory_space=pltpu.VMEM)
    anywhere = pl.BlockSpec(memory_space=pl.ANY)
    all_rows = n * rows
    chips = n // 2
    cols = dense_gate.shape[2]
    others = max(1, n // SPLIT - 1)
    sem = pltpu.SemaphoreType.DMA
    dense_gate = jnp.swapaxes(dense_gate, 1, 2)
    dense_up = jnp.swapaxes(dense_up, 1, 2)
    routes = routes.T
    route_weights = route_weights.T
    results = pl.pallas_call(
        functools.partial(layer_kernel, n),
        name="layer",
        out_shape=(
            jax.ShapeDtypeStruct((rows, width), BF16),
            jax.ShapeDtypeStruct((rows, key_w.shape[1]), BF16),
            jax.ShapeDtypeStruct((rows, value_w.shape[1]), BF16),
        ),
        in_specs=[anywhere] * 21,
        out_specs=(vmem,) * 3,
        scratch_shapes=[
            pltpu.VMEM((rows, width), BF16),
            pltpu.SMEM(lengths.shape, jnp.int32),
            pltpu.SMEM(mix_lambda.shape, F32),
            pltpu.VMEM((1, HEAD_DIM), F32),
            pltpu.VMEM((1, width), F32),
            pltpu.VMEM((1, width), F32),
            pltpu.SMEM(routes.shape, jnp.int32),
            pltpu.SMEM(route_weights.shape, F32),
            pltpu.VMEM((width // SIDE, SIDE), BF16),
            sem((9,)),
            pltpu.VMEM((rows, width + SIDE), BF16),
            pltpu.VMEM((rows, width), F32),
            pltpu.VMEM((rows, span, HEAD_DIM), BF16),
            pltpu.VMEM((rows, span, HEAD_DIM), BF16),
            pltpu.VMEM(query_w.shape, BF16),
            pltpu.VMEM(key_w.shape, BF16),
            pltpu.VMEM(value_w.shape, BF16),
            pltpu.VMEM(out_w.shape, BF16),
            pltpu.VMEM((rows, HEADS, HEAD_DIM), F32),
            pltpu.VMEM((rows, HEADS * HEAD_DIM), F32),
            sem((3 * QKV_CHUNKS,)),
            sem((rows,)),
            sem((rows,)),
            sem((1,)),
            pltpu.VMEM(exp_gate.shape, BF16),
            pltpu.VMEM(exp_up.shape, BF16),
            pltpu.VMEM(exp_down.shape, BF16),
            pltpu.VMEM(dense_gate.shape[1:], BF16),
            pltpu.VMEM(dense_up.shape[1:], BF16),
            pltpu.VMEM(dense_down.shape[1:], BF16),
            pltpu.VMEM((n, rows, width + SIDE), BF16),
            pltpu.VMEM((all_rows, width + SIDE), F32),
            pltpu.VMEM((all_rows, cols), F32),
            pltpu.VMEM((all_rows, cols), F32),
            pltpu.VMEM((all_rows, cols), BF16),
            pltpu.VMEM((all_rows, cols), BF16),
            pltpu.VMEM((others, all_rows, cols), BF16),
            pltpu.VMEM((others, all_rows, cols), BF16),
            pltpu.VMEM((all_rows, exp_gate.shape[1]), BF16),
            pltpu.VMEM((all_rows, width), F32),
            pltpu.VMEM((chips, rows, width), BF16),
            pltpu.VMEM((chips, rows, width), BF16),
            pltpu.VMEM((chips, rows, width), BF16),
            pltpu.VMEM((chips, rows, width), BF16),
            sem((6,)),
            sem((chips,)),
            sem((chips,)),
            sem((chips,)),
            sem((chips,)),
            sem((2 * others * (n // SPLIT),)),
            sem((2 * others * (n // SPLIT),)),
            sem((chips,)),
            sem((chips,)),
            sem((chips,)),
            sem((chips,)),
        ],
        compiler_params=pltpu.CompilerParams(
            collective_id=0, has_side_effects=True, vmem_limit_bytes=63 * 2**20
        ),
    )(
        tokens,
        lengths,
        mix_lambda,
        head_gain.reshape(1, HEAD_DIM),
        attn_gain.reshape(1, width),
        ffn_gain.reshape(1, width),
        routes,
        route_weights,
        branch_gate.reshape(width // SIDE, SIDE),
        cache_keys.reshape(rows, span, HEAD_DIM),
        cache_values.reshape(rows, span, HEAD_DIM),
        query_w,
        key_w,
        value_w,
        out_w,
        exp_gate,
        exp_up,
        exp_down,
        dense_gate,
        dense_up,
        dense_down,
    )
    count = len(results)
    return pl.pallas_call(
        functools.partial(finish_kernel, count),
        name="finish",
        out_shape=tuple(jax.ShapeDtypeStruct(r.shape, r.dtype) for r in results),
        in_specs=[anywhere] * count,
        out_specs=(anywhere,) * count,
        scratch_shapes=[pltpu.VMEM(r.shape, r.dtype) for r in results] + [sem((count,)), sem((count,))],
        compiler_params=pltpu.CompilerParams(vmem_limit_bytes=63 * 2**20),
    )(*results)


def solution(mesh):
    placed = (
        P("ep", None),
        P("ep"),
        P("ep", None, None, None),
        P("ep", None, None, None),
        P(),
        P(),
        P(),
        P(),
        P(),
        P(),
        P(),
        P(),
        P("ep", None),
        P("ep", None),
        P(None, "ep"),
        P(None, "ep"),
        P("ep", None),
        P("ep", None, None),
        P("ep", None, None),
        P("ep", None, None),
        P(),
    )
    return jax.shard_map(
        functools.partial(per_device, mesh.shape["ep"]),
        mesh=mesh,
        in_specs=placed,
        out_specs=(P("ep", None), P("ep", None), P("ep", None)),
        check_vma=False,
    )
```

profile of v0, /device:TPU:0, one launch (start us, length us, event | category | flops | bytes accessed | tf_op | source)
XLA Modules:
  0.0 126.6 jit_solution(10569431750748611338)
XLA Ops:
  0.6 124.6 %layer.1 = (bf16[4,2048]{1,0:T(4,128)(2,1)}, bf16[4,256]{1,0:T(4,128)(2,1)}, bf16[4,256]{1,0:T(4,128)(2,1)}) custom-call(bf16[4,2048]{1,0:T(4,128)(2,1)} %tokens.1, s32[4]{0:T(128)} %lengths.1, f32[8]{0:T(128)} %lam.1, f32[1,128]{1,0:T(1,128)} %bitcast.19, f32[1,2048]{1,0:T(1,128)} %bitcast.14, f32[1,2048]{1,0:T(1,128)} %bitcast.15, s32[2,4]{1,0:T(2,128)} %bitcast.17, ...), custom_call_target="tpu_custom_call" | custom-call | tf_op jit(solution)/shard_map/layer/pallas_call | solution.py:631
  125.2 1.4 %finish.1 = (bf16[4,2048]{1,0:T(4,128)(2,1)}, bf16[4,256]{1,0:T(4,128)(2,1)}, bf16[4,256]{1,0:T(4,128)(2,1)}) custom-call(bf16[4,2048]{1,0:T(4,128)(2,1)} %get-tuple-element.6.refs_0_, bf16[4,256]{1,0:T(4,128)(2,1)} %get-tuple-element.7.refs_1_, bf16[4,256]{1,0:T(4,128)(2,1)} %get-tuple-element.8.refs_2_), custom_call_target="tpu_custom_call" | custom-call | tf_op jit(solution)/shard_map/finish/pallas_call | solution.py:725
where the time goes:
time: 128 us; the launch traced here: 127 us
  Pallas kernels  126 us (98%)
    pallas_call x1, Pallas kernels, per_device(): pl.pallas_call(functools.partial(layer_kernel, n), name='layer', out_shap...  125 us

commit v1 on v0

v1 whole, which is shorter than its diff:
```python
import functools

import jax
import jax.numpy as jnp
from jax import lax
from jax.experimental import pallas as pl
from jax.experimental.pallas import tpu as pltpu
from jax.sharding import PartitionSpec as P

HEADS = 8
KV_HEADS = 2
HEAD_DIM = 128
SPLIT = 16
BLOCKS = 8
EXPERTS = 8
SIDE = 128
QKV_CHUNKS = 4
T = 4
UNITS = 48
GROUP = 8
COLOURS = (("z", "y", "x"), ("x", "y", "z"), ("y", "z", "x"))
IN_COLS = ((0, 768), (768, 1536), (1536, 2176))
OUT_COLS = ((0, 768), (768, 1408), (1408, 2048))

F32 = jnp.float32
BF16 = jnp.bfloat16
MESH = pl.DeviceIdType.MESH


def loop(low, high, body):
    def run(i, carry):
        body(i)
        return carry

    lax.fori_loop(low, high, run, 0)


def silu(v):
    return v / (1.0 + jnp.exp(-v))


def layer_kernel(
    tokens_h,
    lengths_h,
    lam_h,
    head_gain_h,
    attn_gain_h,
    ffn_gain_h,
    routes_h,
    route_weights_h,
    branch_gate_h,
    keys,
    values,
    query_w,
    key_w,
    value_w,
    out_w,
    exp_gate,
    exp_up,
    exp_down,
    dense_gate,
    dense_up,
    dense_down,
    out,
    new_keys,
    new_values,
    tokens,
    lengths,
    lam,
    head_gain,
    attn_gain,
    ffn_gain,
    routes,
    route_weights,
    branch_gate,
    small_sem,
    ext,
    hidden,
    kbuf,
    vbuf,
    qbuf,
    kwbuf,
    vwbuf,
    obuf,
    qscr,
    hscr,
    qkv_sem,
    ksem,
    vsem,
    osem,
    ew,
    dn,
    dgw,
    duw,
    w_sem,
    ws_send,
    ws_recv,
    ds_send,
    ds_recv,
    df_send,
    df_recv,
    recv0,
    recv1,
    recv2,
    side,
    xall,
    act,
    act_perm,
    perm,
    total,
    sendb0,
    sendb1,
    sendb2,
    recvb0,
    recvb1,
    recvb2,
    senda0,
    senda1,
    senda2,
    recva0,
    recva1,
    recva2,
    aga_send,
    aga_recv,
    agb_send,
    agb_recv,
    rsb_send,
    rsb_recv,
    rsa_send,
    rsa_recv,
):
    recv = (recv0, recv1, recv2)
    sendb, recvb = (sendb0, sendb1, sendb2), (recvb0, recvb1, recvb2)
    senda, recva = (senda0, senda1, senda2), (recva0, recva1, recva2)
    rows, width = tokens.shape
    ffn_cols = exp_gate.shape[1]
    all_rows = xall.shape[0]
    span = keys.shape[1]
    step = width // QKV_CHUNKS
    heads_of = HEADS // KV_HEADS
    half = HEAD_DIM // 2
    block_cols = width // BLOCKS

    me = lax.axis_index("ep")
    core = lax.rem(me, 2)
    chip = me // 2
    place = {"z": chip // (T * T), "y": lax.rem(chip // T, T), "x": lax.rem(chip, T)}
    block = me // SPLIT
    expert = block

    def device(at):
        return ((at["z"] * T + at["y"]) * T + at["x"]) * 2 + core

    def mate(c, da, dp, dq):
        at = {name: lax.rem(place[name] + d, T) for name, d in zip(COLOURS[c], (da, dp, dq))}
        return device(at)

    sibling = chip * 2 + 1 - core

    small = [
        pltpu.make_async_copy(src, dst, small_sem.at[i])
        for i, (src, dst) in enumerate(
            (
                (tokens_h, tokens),
                (attn_gain_h, attn_gain),
                (lengths_h, lengths),
                (lam_h, lam),
                (head_gain_h, head_gain),
                (ffn_gain_h, ffn_gain),
                (routes_h, routes),
                (route_weights_h, route_weights),
                (branch_gate_h, branch_gate),
            )
        )
    ]
    for copy in small:
        copy.start()
    weight_copies = []
    for c in range(QKV_CHUNKS):
        part = pl.ds(c * step, step)
        trio = [
            pltpu.make_async_copy(src.at[part], dst.at[part], qkv_sem.at[3 * c + i])
            for i, (src, dst) in enumerate(((query_w, qbuf), (key_w, kwbuf), (value_w, vwbuf)))
        ]
        for copy in trio:
            copy.start()
        weight_copies.append(trio)
    key_copies = [pltpu.make_async_copy(keys.at[s], kbuf.at[s], ksem.at[s]) for s in range(rows)]
    value_copies = [pltpu.make_async_copy(values.at[s], vbuf.at[s], vsem.at[s]) for s in range(rows)]
    for s in range(rows):
        key_copies[s].start()
        value_copies[s].start()
    out_copy = pltpu.make_async_copy(out_w, obuf, osem.at[0])
    out_copy.start()

    gate_cols = pl.ds(pl.multiple_of(core * ffn_cols, 128), ffn_cols)
    up_cols = pl.ds(pl.multiple_of((2 + core) * ffn_cols, 128), ffn_cols)
    down_rows = pl.ds(pl.multiple_of(core * ffn_cols, 128), ffn_cols)
    tile_rows = pl.ds(pl.multiple_of(core * UNITS, 16), UNITS)
    tile_down_rows = pl.ds(pl.multiple_of(2 * ffn_cols + core * UNITS, 16), UNITS)
    tile_cols = pl.ds(pl.multiple_of(block * block_cols, 128), block_cols)

    def window(b):
        return pl.ds(pl.multiple_of(((11 * b) // 2) * GROUP, GROUP), UNITS)

    own_loads = [
        pltpu.make_async_copy(src, dst, w_sem.at[i])
        for i, (src, dst) in enumerate(
            (
                (dense_gate.at[0, window(block)], dgw.at[block, tile_rows]),
                (dense_up.at[0, window(block)], duw.at[block, tile_rows]),
                (dense_down.at[0, window(block)], dn.at[tile_down_rows, tile_cols]),
                (exp_gate, ew.at[:, gate_cols]),
                (exp_up, ew.at[:, up_cols]),
                (exp_down, dn.at[down_rows]),
            )
        )
    ]
    for copy in own_loads:
        copy.start()

    barrier = pltpu.get_barrier_semaphore()
    greeted = 0
    for dz in range(T):
        for dy in range(T):
            for dx in range(T):
                if (dz == 0 or dy == 0 or dx == 0) and (dz, dy, dx) != (0, 0, 0):
                    at = {
                        "z": lax.rem(place["z"] + dz, T),
                        "y": lax.rem(place["y"] + dy, T),
                        "x": lax.rem(place["x"] + dx, T),
                    }
                    pl.semaphore_signal(barrier, inc=1, device_id=(device(at),), device_id_type=MESH)
                    greeted += 1
    pl.semaphore_signal(barrier, inc=1, device_id=(sibling,), device_id_type=MESH)
    greeted += 1

    want = lax.broadcasted_iota(jnp.int32, (all_rows, all_rows), 0)
    have = lax.broadcasted_iota(jnp.int32, (all_rows, all_rows), 1)
    low = have & 3
    first, second, third = (have >> 2) & 3, (have >> 4) & 3, have >> 6
    perm[...] = jnp.where(want == ((first << 6) + (second << 4) + (third << 2) + low), 1.0, 0.0).astype(BF16)
    pad = act.shape[1] - 2 * ffn_cols - 2 * UNITS
    act[:, 2 * ffn_cols + 2 * UNITS :] = jnp.zeros((all_rows, pad), BF16)
    dn[2 * ffn_cols + 2 * UNITS :, :] = jnp.zeros((pad, width), BF16)

    for copy in small:
        copy.wait()

    x = tokens[...].astype(F32)
    normed = x * lax.rsqrt(jnp.mean(x * x, axis=-1, keepdims=True) + 1e-06) * attn_gain[...]
    normed = normed.astype(BF16)
    query = jnp.zeros((rows, query_w.shape[1]), F32)
    knew = jnp.zeros((rows, key_w.shape[1]), F32)
    vnew = jnp.zeros((rows, value_w.shape[1]), F32)
    for c in range(QKV_CHUNKS):
        for copy in weight_copies[c]:
            copy.wait()
        part = slice(c * step, (c + 1) * step)
        left = normed[:, part]
        query += jnp.dot(left, qbuf[part, :], preferred_element_type=F32)
        knew += jnp.dot(left, kwbuf[part, :], preferred_element_type=F32)
        vnew += jnp.dot(left, vwbuf[part, :], preferred_element_type=F32)
    new_keys[...] = knew.astype(BF16)
    new_values[...] = vnew.astype(BF16)
    query = query.astype(BF16).astype(F32)
    knew = knew.astype(BF16).astype(F32)
    vnew = vnew.astype(BF16).astype(F32)
    for s in range(rows):
        for h in range(HEADS):
            qscr[s, h : h + 1, :] = query[s : s + 1, h * HEAD_DIM : (h + 1) * HEAD_DIM]

    pl.semaphore_wait(barrier, greeted)

    def tile_copies(j):
        target = lax.rem(block + j, BLOCKS)
        peer = target * SPLIT + lax.rem(me, SPLIT)
        return [
            pltpu.make_async_remote_copy(
                src_ref=src.at[0, window(target)],
                dst_ref=dst,
                send_sem=ds_send.at[3 * j + i],
                recv_sem=ds_recv.at[3 * j + i],
                device_id=(peer,),
                device_id_type=MESH,
            )
            for i, (src, dst) in enumerate(
                (
                    (dense_gate, dgw.at[block, tile_rows]),
                    (dense_up, duw.at[block, tile_rows]),
                    (dense_down, dn.at[tile_down_rows, tile_cols]),
                )
            )
        ]

    def to_sibling(src, dst, send, recv_sem):
        return pltpu.make_async_remote_copy(
            src_ref=src, dst_ref=dst, send_sem=send, recv_sem=recv_sem, device_id=(sibling,), device_id_type=MESH
        )

    expert_copies = [
        to_sibling(src, dst, ws_send.at[i], ws_recv.at[i])
        for i, (src, dst) in enumerate(
            ((exp_gate, ew.at[:, gate_cols]), (exp_up, ew.at[:, up_cols]), (exp_down, dn.at[down_rows]))
        )
    ]
    tile_forwards = [
        to_sibling(ref, ref, df_send.at[i], df_recv.at[i])
        for i, ref in enumerate((dgw.at[:, tile_rows], duw.at[:, tile_rows], dn.at[tile_down_rows]))
    ]
    for j in range(1, BLOCKS):
        for copy in tile_copies(j):
            copy.start()
    for copy in expert_copies:
        copy.start()

    scale = half ** (-0.5)
    lane = lax.broadcasted_iota(jnp.int32, (HEADS, HEAD_DIM), 1)
    head_row = lax.broadcasted_iota(jnp.int32, (HEADS, HEAD_DIM), 0)
    col = lax.broadcasted_iota(jnp.int32, (2 * HEADS, span), 1)
    row = lax.broadcasted_iota(jnp.int32, (2 * HEADS, span), 0)
    own_group = (col % KV_HEADS) == ((row % HEADS) // heads_of)
    head_col = lax.broadcasted_iota(jnp.int32, (HEADS, 1), 0)
    lam_col = jnp.zeros((HEADS, 1), F32)
    for h in range(HEADS):
        lam_col = jnp.where(head_col == h, lam[h], lam_col)
    for s in range(rows):
        q = qscr[s]
        both = jnp.concatenate([jnp.where(lane < half, q, 0.0), jnp.where(lane >= half, q, 0.0)], axis=0)
        kown = jnp.zeros((HEADS, HEAD_DIM), F32)
        vown = jnp.zeros((HEADS, HEAD_DIM), F32)
        for g in range(KV_HEADS):
            mine = head_row // heads_of == g
            part = slice(g * HEAD_DIM, (g + 1) * HEAD_DIM)
            kown = jnp.where(mine, knew[s : s + 1, part], kown)
            vown = jnp.where(mine, vnew[s : s + 1, part], vown)
        own = jnp.sum(both * jnp.concatenate([kown, kown], axis=0), axis=-1, keepdims=True) * scale
        key_copies[s].wait()
        scores = lax.dot_general(
            both.astype(BF16), kbuf[s], (((1,), (1,)), ((), ())), preferred_element_type=F32
        ) * scale
        valid = own_group & (col < KV_HEADS * lengths[s])
        largest = jnp.maximum(jnp.max(jnp.where(valid, scores, -jnp.inf), axis=-1, keepdims=True), own)
        raised = jnp.where(valid, jnp.exp(scores - largest), 0.0)
        own_raised = jnp.exp(own - largest)
        inverse = 1.0 / (jnp.sum(raised, axis=-1, keepdims=True) + own_raised)
        prob = raised * inverse
        own_prob = own_raised * inverse
        weights = (prob[:HEADS] - lam_col * prob[HEADS:]).astype(BF16)
        own_weights = (own_prob[:HEADS] - lam_col * own_prob[HEADS:]).astype(BF16).astype(F32)
        value_copies[s].wait()
        mixed = jnp.dot(weights, vbuf[s], preferred_element_type=F32) + own_weights * vown
        normal = mixed * lax.rsqrt(jnp.mean(mixed * mixed, axis=-1, keepdims=True) + 1e-05)
        normal = normal * head_gain[...]
        for h in range(HEADS):
            hscr[s : s + 1, h * HEAD_DIM : (h + 1) * HEAD_DIM] = normal[h : h + 1, :]
    out_copy.wait()
    state = x + jnp.dot(hscr[...].astype(BF16), obuf[...], preferred_element_type=F32)
    hidden[...] = state
    ffn = state * lax.rsqrt(jnp.mean(state * state, axis=-1, keepdims=True) + 1e-06)
    ffn = (ffn * ffn_gain[...]).astype(BF16)
    ext[:, :width] = ffn
    pieces = jnp.zeros((rows, SIDE), F32)
    branch = branch_gate[...].astype(F32)
    for c in range(width // SIDE):
        pieces += ffn[:, c * SIDE : (c + 1) * SIDE].astype(F32) * branch[c : c + 1, :]
    logit = jnp.sum(pieces, axis=-1, keepdims=True)
    gate = 1.0 / (1.0 + jnp.exp(-logit))
    spot = lax.broadcasted_iota(jnp.int32, (rows, SIDE), 1)
    name = spot % (SIDE // 2)
    table = jnp.where(name == EXPERTS, gate, 0.0)
    token_row = lax.broadcasted_iota(jnp.int32, (rows, SIDE), 0)
    for k in range(routes.shape[0]):
        for s in range(rows):
            here = (name == routes[k, s]) & (name < EXPERTS) & (token_row == s)
            table = table + jnp.where(here, route_weights[k, s], 0.0)
    high = table.astype(BF16).astype(F32)
    ext[:, width:] = jnp.where(spot < SIDE // 2, high, table - high).astype(BF16)

    def spots(c):
        return [place[name] for name in COLOURS[c]]

    def plane_send(c, dp, dq):
        a, p, q = spots(c)
        i = (c * T + dp) * T + dq
        first, last = IN_COLS[c]
        return pltpu.make_async_remote_copy(
            src_ref=ext.at[:, first:last],
            dst_ref=recv[c].at[(a * T + p) * T + q],
            send_sem=aga_send.at[i],
            recv_sem=aga_recv.at[i],
            device_id=(mate(c, 0, dp, dq),),
            device_id_type=MESH,
        )

    def axis_send(c, da, dp):
        a, p, q = spots(c)
        from_p = lax.rem(p + T - dp, T)
        piece = recv[c].at[pl.ds((a * T + from_p) * T, T)]
        i = (c * (T - 1) + da - 1) * T + dp
        return pltpu.make_async_remote_copy(
            src_ref=piece,
            dst_ref=piece,
            send_sem=agb_send.at[i],
            recv_sem=agb_recv.at[i],
            device_id=(mate(c, da, 0, 0),),
            device_id_type=MESH,
        )

    for dp in (2, 1, 3, 0):
        for dq in (2, 1, 3, 0):
            if (dp, dq) != (0, 0):
                for c in range(3):
                    plane_send(c, dp, dq).start()
    for c in range(3):
        a, p, q = spots(c)
        first, last = IN_COLS[c]
        recv[c][(a * T + p) * T + q] = ext[:, first:last]
    for dp in (0, 1, 3, 2):
        for c in range(3):
            for dq in range(T):
                if (dp, dq) != (0, 0):
                    plane_send(c, dp, dq).wait_recv()
            for da in (2, 1, 3):
                axis_send(c, da, dp).start()
    for copy in own_loads[:3]:
        copy.wait()
    for j in range(1, BLOCKS):
        for copy in tile_copies(j):
            copy.wait_recv()
    for copy in tile_forwards:
        copy.start()

    def widen(z, y):
        group = z * T + y
        at = pl.ds(pl.multiple_of(group * 16, 16), 16)

        def four(ref, spots_of, cols):
            return jnp.concatenate([ref[i, :, cols].astype(F32) for i in spots_of], axis=0)

        one = four(recv0, [group * T + i for i in range(T)], slice(None))
        xall[at, IN_COLS[0][0] : IN_COLS[0][1]] = one.astype(BF16)
        one = four(recv1, [(i * T + y) * T + z for i in range(T)], slice(None))
        xall[at, IN_COLS[1][0] : IN_COLS[1][1]] = one.astype(BF16)
        where = [(y * T + z) * T + i for i in range(T)]
        one = four(recv2, where, slice(0, width - IN_COLS[2][0]))
        xall[at, IN_COLS[2][0] : width] = one.astype(BF16)
        side[at, :] = four(recv2, where, slice(width - IN_COLS[2][0], None))

    for da in (1, 3, 2):
        for dp in (0, 1, 3, 2):
            for c in range(3):
                axis_send(c, da, dp).wait_recv()
    loop(0, T * T, lambda i: widen(i // T, lax.rem(i, T)))

    for copy in own_loads[3:]:
        copy.wait()
    for copy in expert_copies:
        copy.wait_recv()

    spot = lax.broadcasted_iota(jnp.int32, side.shape, 1) % (SIDE // 2)
    table = side[...]
    routed = jnp.sum(jnp.where(spot == expert, table, 0.0), axis=-1, keepdims=True)
    gate = jnp.sum(jnp.where(spot == EXPERTS, table, 0.0), axis=-1, keepdims=True)
    hid = 2 * ffn_cols
    for n in range(hid // 256):
        cols = slice(n * 256, (n + 1) * 256)
        g = jnp.dot(xall[...], ew[:, cols], preferred_element_type=F32)
        u = jnp.dot(xall[...], ew[:, hid + n * 256 : hid + (n + 1) * 256], preferred_element_type=F32)
        act[:, cols] = (silu(g) * u * routed).astype(BF16)
    for copy in tile_forwards:
        copy.wait_recv()
    across = (((1,), (1,)), ((), ()))
    g = jnp.zeros((all_rows, 2 * UNITS), F32)
    u = jnp.zeros((all_rows, 2 * UNITS), F32)
    for b in range(BLOCKS):
        left = xall[:, b * block_cols : (b + 1) * block_cols]
        g += lax.dot_general(left, dgw[b], across, preferred_element_type=F32)
        u += lax.dot_general(left, duw[b], across, preferred_element_type=F32)
    unit = lax.broadcasted_iota(jnp.int32, g.shape, 1)
    unit = jnp.where(unit >= UNITS, unit - UNITS, unit)
    taken = UNITS - GROUP * (1 - lax.rem(block, 2))
    dact = jnp.where(unit < taken, silu(g) * u * gate, 0.0)
    act[:, hid : hid + 2 * UNITS] = dact.astype(BF16)
    act_perm[...] = jnp.dot(perm[...], act[...], preferred_element_type=F32).astype(BF16)

    def slab(c, a, p):
        return p * T + a if c == 2 else a * T + p

    def axis_sum(c, da, k):
        a, p, q = spots(c)
        i = (c * (T - 1) + da - 1) * T + k
        return pltpu.make_async_remote_copy(
            src_ref=sendb[c].at[slab(c, lax.rem(a + da, T), lax.rem(p + k, T))],
            dst_ref=recvb[c].at[(da - 1) * T + k],
            send_sem=rsb_send.at[i],
            recv_sem=rsb_recv.at[i],
            device_id=(mate(c, da, 0, 0),),
            device_id_type=MESH,
        )

    def plane_sum(c, k, l):
        a, p, q = spots(c)
        i = (c * T + k) * T + l
        return pltpu.make_async_remote_copy(
            src_ref=senda[c].at[lax.rem(p + k, T) * T + lax.rem(q + l, T)],
            dst_ref=recva[c].at[k * T + l],
            send_sem=rsa_send.at[i],
            recv_sem=rsa_recv.at[i],
            device_id=(mate(c, 0, k, l),),
            device_id_type=MESH,
        )

    for c in range(3):
        first, last = OUT_COLS[c]
        left = act_perm if c == 1 else act
        part = jnp.dot(left[...], dn[:, first:last], preferred_element_type=F32)
        total[:, first:last] = part
        for i in range(T * T):
            sendb[c][i] = part[i * 16 : (i + 1) * 16].astype(BF16)
        for k in (2, 1, 3, 0):
            for da in (2, 1, 3):
                axis_sum(c, da, k).start()

    for c in range(3):
        for dp in range(T):
            for dq in range(T):
                if (dp, dq) != (0, 0):
                    plane_send(c, dp, dq).wait_send()
        for da in range(1, T):
            for dp in range(T):
                axis_send(c, da, dp).wait_send()
    for j in range(1, BLOCKS):
        for copy in tile_copies(j):
            copy.wait_send()
    for copy in expert_copies:
        copy.wait_send()
    for copy in tile_forwards:
        copy.wait_send()

    for k in (2, 1, 3, 0):
        for c in range(3):
            a, p, q = spots(c)
            first, last = OUT_COLS[c]
            row16 = pl.ds(pl.multiple_of(slab(c, a, lax.rem(p + k, T)) * 16, 16), 16)
            acc = total[row16, first:last]
            for da in (1, 3, 2):
                axis_sum(c, da, k).wait_recv()
                acc = acc + recvb[c][(da - 1) * T + k].astype(F32)
            for i in range(T):
                senda[c][lax.rem(p + k, T) * T + i] = acc[i * rows : (i + 1) * rows].astype(BF16)
            for l in (2, 1, 3, 0):
                if (k, l) != (0, 0):
                    plane_sum(c, k, l).start()
    for c in range(3):
        for da in range(1, T):
            for k in range(T):
                axis_sum(c, da, k).wait_send()
    for c in range(3):
        a, p, q = spots(c)
        first, last = OUT_COLS[c]
        acc = hidden[:, first:last] + senda[c][p * T + q].astype(F32)
        for k in (0, 1, 3, 2):
            for l in (0, 1, 3, 2):
                if (k, l) != (0, 0):
                    plane_sum(c, k, l).wait_recv()
                    acc = acc + recva[c][k * T + l].astype(F32)
        out[:, first:last] = acc.astype(BF16)
    for c in range(3):
        for k in range(T):
            for l in range(T):
                if (k, l) != (0, 0):
                    plane_sum(c, k, l).wait_send()


def finish_kernel(count, *refs):
    sources, targets, held = refs[:count], refs[count : 2 * count], refs[2 * count : 3 * count]
    in_sem, out_sem = refs[3 * count :]
    ins = [pltpu.make_async_copy(sources[i], held[i], in_sem.at[i]) for i in range(count)]
    outs = [pltpu.make_async_copy(held[i], targets[i], out_sem.at[i]) for i in range(count)]
    for copy in ins:
        copy.start()
    for i in range(count):
        ins[i].wait()
        outs[i].start()
    for copy in outs:
        copy.wait()


def per_device(
    tokens,
    lengths,
    cache_keys,
    cache_values,
    query_w,
    key_w,
    value_w,
    out_w,
    mix_lambda,
    head_gain,
    attn_gain,
    ffn_gain,
    routes,
    route_weights,
    exp_gate,
    exp_up,
    exp_down,
    dense_gate,
    dense_up,
    dense_down,
    branch_gate,
):
    rows, width = tokens.shape
    span = cache_keys.shape[1] * KV_HEADS
    vmem = pl.BlockSpec(memory_space=pltpu.VMEM)
    anywhere = pl.BlockSpec(memory_space=pl.ANY)
    chips = T * T * T
    all_rows = chips * rows
    hid = 2 * exp_gate.shape[1]
    padded = -(-(hid + 2 * UNITS) // 128) * 128
    block_cols = width // BLOCKS
    sem = pltpu.SemaphoreType.DMA
    dense_gate = jnp.swapaxes(dense_gate, 1, 2)
    dense_up = jnp.swapaxes(dense_up, 1, 2)
    routes = routes.T
    route_weights = route_weights.T
    in_cols = [last - first for first, last in IN_COLS]
    out_cols = [last - first for first, last in OUT_COLS]
    results = pl.pallas_call(
        layer_kernel,
        name="layer",
        out_shape=(
            jax.ShapeDtypeStruct((rows, width), BF16),
            jax.ShapeDtypeStruct((rows, key_w.shape[1]), BF16),
            jax.ShapeDtypeStruct((rows, value_w.shape[1]), BF16),
        ),
        in_specs=[anywhere] * 21,
        out_specs=(vmem,) * 3,
        scratch_shapes=[
            pltpu.VMEM((rows, width), BF16),
            pltpu.SMEM(lengths.shape, jnp.int32),
            pltpu.SMEM(mix_lambda.shape, F32),
            pltpu.VMEM((1, HEAD_DIM), F32),
            pltpu.VMEM((1, width), F32),
            pltpu.VMEM((1, width), F32),
            pltpu.SMEM(routes.shape, jnp.int32),
            pltpu.SMEM(route_weights.shape, F32),
            pltpu.VMEM((width // SIDE, SIDE), BF16),
            sem((9,)),
            pltpu.VMEM((rows, width + SIDE), BF16),
            pltpu.VMEM((rows, width), F32),
            pltpu.VMEM((rows, span, HEAD_DIM), BF16),
            pltpu.VMEM((rows, span, HEAD_DIM), BF16),
            pltpu.VMEM(query_w.shape, BF16),
            pltpu.VMEM(key_w.shape, BF16),
            pltpu.VMEM(value_w.shape, BF16),
            pltpu.VMEM(out_w.shape, BF16),
            pltpu.VMEM((rows, HEADS, HEAD_DIM), F32),
            pltpu.VMEM((rows, HEADS * HEAD_DIM), F32),
            sem((3 * QKV_CHUNKS,)),
            sem((rows,)),
            sem((rows,)),
            sem((1,)),
            pltpu.VMEM((width, 2 * hid), BF16),
            pltpu.VMEM((padded, width), BF16),
            pltpu.VMEM((BLOCKS, 2 * UNITS, block_cols), BF16),
            pltpu.VMEM((BLOCKS, 2 * UNITS, block_cols), BF16),
            sem((6,)),
            sem((3,)),
            sem((3,)),
            sem((3 * BLOCKS,)),
            sem((3 * BLOCKS,)),
            sem((3,)),
            sem((3,)),
        ]
        + [pltpu.VMEM((chips, rows, cols), BF16) for cols in in_cols]
        + [
            pltpu.VMEM((all_rows, SIDE), F32),
            pltpu.VMEM((all_rows, width), BF16),
            pltpu.VMEM((all_rows, padded), BF16),
            pltpu.VMEM((all_rows, padded), BF16),
            pltpu.VMEM((all_rows, all_rows), BF16),
            pltpu.VMEM((all_rows, width), F32),
        ]
        + [pltpu.VMEM((T * T, T * rows, cols), BF16) for cols in out_cols]
        + [pltpu.VMEM(((T - 1) * T, T * rows, cols), BF16) for cols in out_cols]
        + [pltpu.VMEM((T * T, rows, cols), BF16) for cols in out_cols]
        + [pltpu.VMEM((T * T, rows, cols), BF16) for cols in out_cols]
        + [
            sem((3 * T * T,)),
            sem((3 * T * T,)),
            sem((3 * (T - 1) * T,)),
            sem((3 * (T - 1) * T,)),
            sem((3 * (T - 1) * T,)),
            sem((3 * (T - 1) * T,)),
            sem((3 * T * T,)),
            sem((3 * T * T,)),
        ],
        compiler_params=pltpu.CompilerParams(
            collective_id=0, has_side_effects=True, vmem_limit_bytes=63 * 2**20
        ),
    )(
        tokens,
        lengths,
        mix_lambda,
        head_gain.reshape(1, HEAD_DIM),
        attn_gain.reshape(1, width),
        ffn_gain.reshape(1, width),
        routes,
        route_weights,
        branch_gate.reshape(width // SIDE, SIDE),
        cache_keys.reshape(rows, span, HEAD_DIM),
        cache_values.reshape(rows, span, HEAD_DIM),
        query_w,
        key_w,
        value_w,
        out_w,
        exp_gate,
        exp_up,
        exp_down,
        dense_gate,
        dense_up,
        dense_down,
    )
    count = len(results)
    return pl.pallas_call(
        functools.partial(finish_kernel, count),
        name="finish",
        out_shape=tuple(jax.ShapeDtypeStruct(r.shape, r.dtype) for r in results),
        in_specs=[anywhere] * count,
        out_specs=(anywhere,) * count,
        scratch_shapes=[pltpu.VMEM(r.shape, r.dtype) for r in results] + [sem((count,)), sem((count,))],
        compiler_params=pltpu.CompilerParams(vmem_limit_bytes=63 * 2**20),
    )(*results)


def solution(mesh):
    placed = (
        P("ep", None),
        P("ep"),
        P("ep", None, None, None),
        P("ep", None, None, None),
        P(),
        P(),
        P(),
        P(),
        P(),
        P(),
        P(),
        P(),
        P("ep", None),
        P("ep", None),
        P(None, "ep"),
        P(None, "ep"),
        P("ep", None),
        P("ep", None, None),
        P("ep", None, None),
        P("ep", None, None),
        P(),
    )
    return jax.shard_map(
        per_device,
        mesh=mesh,
        in_specs=placed,
        out_specs=(P("ep", None), P("ep", None), P("ep", None)),
        check_vma=False,
    )
```

time: 128 us -> 48.3 us (0.38)
  Pallas kernels: 126 us -> 47.5 us
    pallas_call x1, Pallas kernels: 125 us -> 46.1 us  [per_device(): pl.pallas_call(layer_kernel, name='layer', out_shape=(jax.ShapeDtypeStruc...]
where the time goes in v1:
time: 48.3 us; the launch traced here: 48.1 us
  Pallas kernels  47.5 us (98%)
  between operations  0.65 us (1%)
    pallas_call x1, Pallas kernels, per_device(): pl.pallas_call(layer_kernel, name='layer', out_shape=(jax.ShapeDtypeStruc...  46.1 us
    pallas_call x1, Pallas kernels, per_device(): pl.pallas_call(functools.partial(finish_kernel, count), name='finish', ou...  1.38 us

profile of v1, /device:TPU:0, one launch (start us, length us, event | category | flops | bytes accessed | tf_op | source)
XLA Modules:
  0.0 48.1 jit_solution(366133923627829441)
XLA Ops:
  0.6 46.1 %layer.1 = (bf16[4,2048]{1,0:T(4,128)(2,1)}, bf16[4,256]{1,0:T(4,128)(2,1)}, bf16[4,256]{1,0:T(4,128)(2,1)}) custom-call(bf16[4,2048]{1,0:T(4,128)(2,1)} %tokens_h.1, s32[4]{0:T(128)} %lengths_h.1, f32[8]{0:T(128)} %lam_h.1, f32[1,128]{1,0:T(1,128)} %bitcast.19, f32[1,2048]{1,0:T(1,128)} %bitcast.14, f32[1,2048]{1,0:T(1,128)} %bitcast.15, s32[2,4]{1,0:T(2,128)} %bitcast.17, ...), custom_call_target="tpu_custom_call" | custom-call | tf_op jit(solution)/shard_map/layer/pallas_call | solution.py:629
  46.8 1.4 %finish.1 = (bf16[4,2048]{1,0:T(4,128)(2,1)}, bf16[4,256]{1,0:T(4,128)(2,1)}, bf16[4,256]{1,0:T(4,128)(2,1)}) custom-call(bf16[4,2048]{1,0:T(4,128)(2,1)} %get-tuple-element.6.refs_0_, bf16[4,256]{1,0:T(4,128)(2,1)} %get-tuple-element.7.refs_1_, bf16[4,256]{1,0:T(4,128)(2,1)} %get-tuple-element.8.refs_2_), custom_call_target="tpu_custom_call" | custom-call | tf_op jit(solution)/shard_map/finish/pallas_call | solution.py:726

commit v2 on v1

--- a/solution.py
+++ b/solution.py
@@ -107,7 +107,6 @@
     act,
     act_perm,
     perm,
-    total,
     sendb0,
     sendb1,
     sendb2,
@@ -187,11 +186,7 @@
         weight_copies.append(trio)
     key_copies = [pltpu.make_async_copy(keys.at[s], kbuf.at[s], ksem.at[s]) for s in range(rows)]
     value_copies = [pltpu.make_async_copy(values.at[s], vbuf.at[s], vsem.at[s]) for s in range(rows)]
-    for s in range(rows):
-        key_copies[s].start()
-        value_copies[s].start()
     out_copy = pltpu.make_async_copy(out_w, obuf, osem.at[0])
-    out_copy.start()
 
     gate_cols = pl.ds(pl.multiple_of(core * ffn_cols, 128), ffn_cols)
     up_cols = pl.ds(pl.multiple_of((2 + core) * ffn_cols, 128), ffn_cols)
@@ -216,8 +211,6 @@
             )
         )
     ]
-    for copy in own_loads:
-        copy.start()
 
     barrier = pltpu.get_barrier_semaphore()
     greeted = 0
@@ -244,9 +237,10 @@
     act[:, 2 * ffn_cols + 2 * UNITS :] = jnp.zeros((all_rows, pad), BF16)
     dn[2 * ffn_cols + 2 * UNITS :, :] = jnp.zeros((pad, width), BF16)
 
-    for copy in small:
-        copy.wait()
-
+    small[0].wait()
+    small[1].wait()
+    for copy in key_copies + value_copies:
+        copy.start()
     x = tokens[...].astype(F32)
     normed = x * lax.rsqrt(jnp.mean(x * x, axis=-1, keepdims=True) + 1e-06) * attn_gain[...]
     normed = normed.astype(BF16)
@@ -270,6 +264,9 @@
         for h in range(HEADS):
             qscr[s, h : h + 1, :] = query[s : s + 1, h * HEAD_DIM : (h + 1) * HEAD_DIM]
 
+    out_copy.start()
+    for copy in own_loads:
+        copy.start()
     pl.semaphore_wait(barrier, greeted)
 
     def tile_copies(j):
@@ -279,8 +276,8 @@
             pltpu.make_async_remote_copy(
                 src_ref=src.at[0, window(target)],
                 dst_ref=dst,
-                send_sem=ds_send.at[3 * j + i],
-                recv_sem=ds_recv.at[3 * j + i],
+                send_sem=ds_send.at[i],
+                recv_sem=ds_recv.at[i],
                 device_id=(peer,),
                 device_id_type=MESH,
             )
@@ -293,6 +290,13 @@
             )
         ]
 
+    def stand_in(ref, send, recv_sem):
+        return pltpu.make_async_remote_copy(
+            src_ref=ref, dst_ref=ref, send_sem=send, recv_sem=recv_sem, device_id=(sibling,), device_id_type=MESH
+        )
+
+    all_tiles = [stand_in(dgw.at[: BLOCKS - 1, :UNITS], ds_send.at[i], ds_recv.at[i]) for i in range(3)]
+
     def to_sibling(src, dst, send, recv_sem):
         return pltpu.make_async_remote_copy(
             src_ref=src, dst_ref=dst, send_sem=send, recv_sem=recv_sem, device_id=(sibling,), device_id_type=MESH
@@ -314,6 +318,8 @@
     for copy in expert_copies:
         copy.start()
 
+    for copy in small[2:]:
+        copy.wait()
     scale = half ** (-0.5)
     lane = lax.broadcasted_iota(jnp.int32, (HEADS, HEAD_DIM), 1)
     head_row = lax.broadcasted_iota(jnp.int32, (HEADS, HEAD_DIM), 0)
@@ -324,6 +330,9 @@
     lam_col = jnp.zeros((HEADS, 1), F32)
     for h in range(HEADS):
         lam_col = jnp.where(head_col == h, lam[h], lam_col)
+    for copy in key_copies:
+        copy.wait()
+    scores, owns, vowns = [], [], []
     for s in range(rows):
         q = qscr[s]
         both = jnp.concatenate([jnp.where(lane < half, q, 0.0), jnp.where(lane >= half, q, 0.0)], axis=0)
@@ -334,22 +343,27 @@
             part = slice(g * HEAD_DIM, (g + 1) * HEAD_DIM)
             kown = jnp.where(mine, knew[s : s + 1, part], kown)
             vown = jnp.where(mine, vnew[s : s + 1, part], vown)
-        own = jnp.sum(both * jnp.concatenate([kown, kown], axis=0), axis=-1, keepdims=True) * scale
-        key_copies[s].wait()
-        scores = lax.dot_general(
-            both.astype(BF16), kbuf[s], (((1,), (1,)), ((), ())), preferred_element_type=F32
-        ) * scale
+        owns.append(jnp.sum(both * jnp.concatenate([kown, kown], axis=0), axis=-1, keepdims=True) * scale)
+        vowns.append(vown)
+        scores.append(
+            lax.dot_general(both.astype(BF16), kbuf[s], (((1,), (1,)), ((), ())), preferred_element_type=F32)
+        )
+    weights, own_weights = [], []
+    for s in range(rows):
         valid = own_group & (col < KV_HEADS * lengths[s])
-        largest = jnp.maximum(jnp.max(jnp.where(valid, scores, -jnp.inf), axis=-1, keepdims=True), own)
-        raised = jnp.where(valid, jnp.exp(scores - largest), 0.0)
-        own_raised = jnp.exp(own - largest)
+        scaled = jnp.where(valid, scores[s] * scale, -jnp.inf)
+        largest = jnp.maximum(jnp.max(scaled, axis=-1, keepdims=True), owns[s])
+        raised = jnp.exp(scaled - largest)
+        own_raised = jnp.exp(owns[s] - largest)
         inverse = 1.0 / (jnp.sum(raised, axis=-1, keepdims=True) + own_raised)
         prob = raised * inverse
         own_prob = own_raised * inverse
-        weights = (prob[:HEADS] - lam_col * prob[HEADS:]).astype(BF16)
-        own_weights = (own_prob[:HEADS] - lam_col * own_prob[HEADS:]).astype(BF16).astype(F32)
-        value_copies[s].wait()
-        mixed = jnp.dot(weights, vbuf[s], preferred_element_type=F32) + own_weights * vown
+        weights.append((prob[:HEADS] - lam_col * prob[HEADS:]).astype(BF16))
+        own_weights.append((own_prob[:HEADS] - lam_col * own_prob[HEADS:]).astype(BF16).astype(F32))
+    for copy in value_copies:
+        copy.wait()
+    for s in range(rows):
+        mixed = jnp.dot(weights[s], vbuf[s], preferred_element_type=F32) + own_weights[s] * vowns[s]
         normal = mixed * lax.rsqrt(jnp.mean(mixed * mixed, axis=-1, keepdims=True) + 1e-05)
         normal = normal * head_gain[...]
         for h in range(HEADS):
@@ -382,13 +396,12 @@
 
     def plane_send(c, dp, dq):
         a, p, q = spots(c)
-        i = (c * T + dp) * T + dq
         first, last = IN_COLS[c]
         return pltpu.make_async_remote_copy(
             src_ref=ext.at[:, first:last],
             dst_ref=recv[c].at[(a * T + p) * T + q],
-            send_sem=aga_send.at[i],
-            recv_sem=aga_recv.at[i],
+            send_sem=aga_send.at[c],
+            recv_sem=aga_recv.at[c * T + dp],
             device_id=(mate(c, 0, dp, dq),),
             device_id_type=MESH,
         )
@@ -397,12 +410,11 @@
         a, p, q = spots(c)
         from_p = lax.rem(p + T - dp, T)
         piece = recv[c].at[pl.ds((a * T + from_p) * T, T)]
-        i = (c * (T - 1) + da - 1) * T + dp
         return pltpu.make_async_remote_copy(
             src_ref=piece,
             dst_ref=piece,
-            send_sem=agb_send.at[i],
-            recv_sem=agb_recv.at[i],
+            send_sem=agb_send.at[c],
+            recv_sem=agb_recv.at[c],
             device_id=(mate(c, da, 0, 0),),
             device_id_type=MESH,
         )
@@ -418,16 +430,14 @@
         recv[c][(a * T + p) * T + q] = ext[:, first:last]
     for dp in (0, 1, 3, 2):
         for c in range(3):
-            for dq in range(T):
-                if (dp, dq) != (0, 0):
-                    plane_send(c, dp, dq).wait_recv()
+            ref = recv[c].at[: T - 1 if dp == 0 else T]
+            stand_in(ref, aga_send.at[c], aga_recv.at[c * T + dp]).wait_recv()
             for da in (2, 1, 3):
                 axis_send(c, da, dp).start()
     for copy in own_loads[:3]:
         copy.wait()
-    for j in range(1, BLOCKS):
-        for copy in tile_copies(j):
-            copy.wait_recv()
+    for copy in all_tiles:
+        copy.wait_recv()
     for copy in tile_forwards:
         copy.start()
 
@@ -447,10 +457,8 @@
         xall[at, IN_COLS[2][0] : width] = one.astype(BF16)
         side[at, :] = four(recv2, where, slice(width - IN_COLS[2][0], None))
 
-    for da in (1, 3, 2):
-        for dp in (0, 1, 3, 2):
-            for c in range(3):
-                axis_send(c, da, dp).wait_recv()
+    for c in range(3):
+        stand_in(recv[c].at[: (T - 1) * T * T], agb_send.at[c], agb_recv.at[c]).wait_recv()
     loop(0, T * T, lambda i: widen(i // T, lax.rem(i, T)))
 
     for copy in own_loads[3:]:
@@ -489,24 +497,22 @@
 
     def axis_sum(c, da, k):
         a, p, q = spots(c)
-        i = (c * (T - 1) + da - 1) * T + k
         return pltpu.make_async_remote_copy(
             src_ref=sendb[c].at[slab(c, lax.rem(a + da, T), lax.rem(p + k, T))],
-            dst_ref=recvb[c].at[(da - 1) * T + k],
-            send_sem=rsb_send.at[i],
-            recv_sem=rsb_recv.at[i],
+            dst_ref=recvb[c].at[k * (T - 1) + da - 1],
+            send_sem=rsb_send.at[c],
+            recv_sem=rsb_recv.at[c * T + k],
             device_id=(mate(c, da, 0, 0),),
             device_id_type=MESH,
         )
 
     def plane_sum(c, k, l):
         a, p, q = spots(c)
-        i = (c * T + k) * T + l
         return pltpu.make_async_remote_copy(
             src_ref=senda[c].at[lax.rem(p + k, T) * T + lax.rem(q + l, T)],
-            dst_ref=recva[c].at[k * T + l],
-            send_sem=rsa_send.at[i],
-            recv_sem=rsa_recv.at[i],
+            dst_ref=recva[c].at[k * T + l - 1],
+            send_sem=rsa_send.at[c],
+            recv_sem=rsa_recv.at[c],
             device_id=(mate(c, 0, k, l),),
             device_id_type=MESH,
         )
@@ -515,7 +521,6 @@
         first, last = OUT_COLS[c]
         left = act_perm if c == 1 else act
         part = jnp.dot(left[...], dn[:, first:last], preferred_element_type=F32)
-        total[:, first:last] = part
         for i in range(T * T):
             sendb[c][i] = part[i * 16 : (i + 1) * 16].astype(BF16)
         for k in (2, 1, 3, 0):
@@ -523,16 +528,10 @@
                 axis_sum(c, da, k).start()
 
     for c in range(3):
-        for dp in range(T):
-            for dq in range(T):
-                if (dp, dq) != (0, 0):
-                    plane_send(c, dp, dq).wait_send()
-        for da in range(1, T):
-            for dp in range(T):
-                axis_send(c, da, dp).wait_send()
-    for j in range(1, BLOCKS):
-        for copy in tile_copies(j):
-            copy.wait_send()
+        stand_in(recv[c].at[: T * T - 1], aga_send.at[c], aga_recv.at[c * T]).wait_send()
+        stand_in(recv[c].at[: (T - 1) * T * T], agb_send.at[c], agb_recv.at[c]).wait_send()
+    for copy in all_tiles:
+        copy.wait_send()
     for copy in expert_copies:
         copy.wait_send()
     for copy in tile_forwards:
@@ -541,36 +540,27 @@
     for k in (2, 1, 3, 0):
         for c in range(3):
             a, p, q = spots(c)
-            first, last = OUT_COLS[c]
-            row16 = pl.ds(pl.multiple_of(slab(c, a, lax.rem(p + k, T)) * 16, 16), 16)
-            acc = total[row16, first:last]
-            for da in (1, 3, 2):
-                axis_sum(c, da, k).wait_recv()
-                acc = acc + recvb[c][(da - 1) * T + k].astype(F32)
+            stand_in(recvb[c].at[: T - 1], rsb_send.at[c], rsb_recv.at[c * T + k]).wait_recv()
+            acc = sendb[c][slab(c, a, lax.rem(p + k, T))].astype(F32)
+            for i in range(T - 1):
+                acc = acc + recvb[c][k * (T - 1) + i].astype(F32)
             for i in range(T):
                 senda[c][lax.rem(p + k, T) * T + i] = acc[i * rows : (i + 1) * rows].astype(BF16)
             for l in (2, 1, 3, 0):
                 if (k, l) != (0, 0):
                     plane_sum(c, k, l).start()
     for c in range(3):
-        for da in range(1, T):
-            for k in range(T):
-                axis_sum(c, da, k).wait_send()
+        stand_in(sendb[c].at[: (T - 1) * T], rsb_send.at[c], rsb_recv.at[c * T]).wait_send()
     for c in range(3):
         a, p, q = spots(c)
         first, last = OUT_COLS[c]
         acc = hidden[:, first:last] + senda[c][p * T + q].astype(F32)
-        for k in (0, 1, 3, 2):
-            for l in (0, 1, 3, 2):
-                if (k, l) != (0, 0):
-                    plane_sum(c, k, l).wait_recv()
-                    acc = acc + recva[c][k * T + l].astype(F32)
+        stand_in(recva[c].at[: T * T - 1], rsa_send.at[c], rsa_recv.at[c]).wait_recv()
+        for i in range(T * T - 1):
+            acc = acc + recva[c][i].astype(F32)
         out[:, first:last] = acc.astype(BF16)
     for c in range(3):
-        for k in range(T):
-            for l in range(T):
-                if (k, l) != (0, 0):
-                    plane_sum(c, k, l).wait_send()
+        stand_in(senda[c].at[: T * T - 1], rsa_send.at[c], rsa_recv.at[c]).wait_send()
 
 
 def finish_kernel(count, *refs):
@@ -668,8 +658,8 @@
             sem((6,)),
             sem((3,)),
             sem((3,)),
-            sem((3 * BLOCKS,)),
-            sem((3 * BLOCKS,)),
+            sem((3,)),
+            sem((3,)),
             sem((3,)),
             sem((3,)),
         ]
@@ -680,21 +670,20 @@
             pltpu.VMEM((all_rows, padded), BF16),
             pltpu.VMEM((all_rows, padded), BF16),
             pltpu.VMEM((all_rows, all_rows), BF16),
-            pltpu.VMEM((all_rows, width), F32),
         ]
         + [pltpu.VMEM((T * T, T * rows, cols), BF16) for cols in out_cols]
         + [pltpu.VMEM(((T - 1) * T, T * rows, cols), BF16) for cols in out_cols]
         + [pltpu.VMEM((T * T, rows, cols), BF16) for cols in out_cols]
-        + [pltpu.VMEM((T * T, rows, cols), BF16) for cols in out_cols]
+        + [pltpu.VMEM((T * T - 1, rows, cols), BF16) for cols in out_cols]
         + [
-            sem((3 * T * T,)),
-            sem((3 * T * T,)),
-            sem((3 * (T - 1) * T,)),
-            sem((3 * (T - 1) * T,)),
-            sem((3 * (T - 1) * T,)),
-            sem((3 * (T - 1) * T,)),
-            sem((3 * T * T,)),
-            sem((3 * T * T,)),
+            sem((3,)),
+            sem((3 * T,)),
+            sem((3,)),
+            sem((3,)),
+            sem((3,)),
+            sem((3 * T,)),
+            sem((3,)),
+            sem((3,)),
         ],
         compiler_params=pltpu.CompilerParams(
             collective_id=0, has_side_effects=True, vmem_limit_bytes=63 * 2**20

time: 48.3 us -> 43.5 us (0.901)
  Pallas kernels: 47.5 us -> 42.6 us
    pallas_call x1, Pallas kernels: 46.1 us -> 41.3 us  [per_device(): pl.pallas_call(layer_kernel, name='layer', out_shape=(jax.ShapeDtypeStruc...]
where the time goes in v2:
time: 43.5 us; the launch traced here: 43.3 us
  Pallas kernels  42.6 us (98%)
  between operations  0.65 us (1%)
    pallas_call x1, Pallas kernels, per_device(): pl.pallas_call(layer_kernel, name='layer', out_shape=(jax.ShapeDtypeStruc...  41.3 us
    pallas_call x1, Pallas kernels, per_device(): pl.pallas_call(functools.partial(finish_kernel, count), name='finish', ou...  1.38 us

profile of v2, /device:TPU:0, one launch (start us, length us, event | category | flops | bytes accessed | tf_op | source)
XLA Modules:
  0.0 43.3 jit_solution(14645804003753734385)
XLA Ops:
  0.6 41.3 %layer.1 = (bf16[4,2048]{1,0:T(4,128)(2,1)}, bf16[4,256]{1,0:T(4,128)(2,1)}, bf16[4,256]{1,0:T(4,128)(2,1)}) custom-call(bf16[4,2048]{1,0:T(4,128)(2,1)} %tokens_h.1, s32[4]{0:T(128)} %lengths_h.1, f32[8]{0:T(128)} %lam_h.1, f32[1,128]{1,0:T(1,128)} %bitcast.19, f32[1,2048]{1,0:T(1,128)} %bitcast.14, f32[1,2048]{1,0:T(1,128)} %bitcast.15, s32[2,4]{1,0:T(2,128)} %bitcast.17, ...), custom_call_target="tpu_custom_call" | custom-call | tf_op jit(solution)/shard_map/layer/pallas_call | solution.py:619
  41.9 1.4 %finish.1 = (bf16[4,2048]{1,0:T(4,128)(2,1)}, bf16[4,256]{1,0:T(4,128)(2,1)}, bf16[4,256]{1,0:T(4,128)(2,1)}) custom-call(bf16[4,2048]{1,0:T(4,128)(2,1)} %get-tuple-element.6.refs_0_, bf16[4,256]{1,0:T(4,128)(2,1)} %get-tuple-element.7.refs_1_, bf16[4,256]{1,0:T(4,128)(2,1)} %get-tuple-element.8.refs_2_), custom_call_target="tpu_custom_call" | custom-call | tf_op jit(solution)/shard_map/finish/pallas_call | solution.py:715
